TPU v7x, 32 devices: a whole 2x2x4 slice. The times are simulated.
32 devices in a mesh: tp: 8 (over z, x), dp: 4 (over y, core).
Axes of the slice: x: 2, y: 2, z: 4, core: 2. Of those that a mesh axis runs over, the one named last changes fastest.
Arguments:
- tokens: bfloat16 [128, 8, 4096], P('dp', None, 'tp'), may hold values from -12 to 12
- lengths: int32 [128], P('dp'), may hold values from 1 to 8, 384 in all
- norm_gains: float32 [2, 4096], replicated, may hold values from 0.1 to 1.9
- drive_proj: bfloat16 [2, 4096, 2048], P(None, 'dp', 'tp'), may hold values from -0.09375 to 0.09375
- open_proj: bfloat16 [2, 4096, 4096], P(None, 'dp', 'tp'), may hold values from -0.09375 to 0.09375
- glu_proj: bfloat16 [2, 2048, 2048], P(None, 'dp', 'tp'), may hold values from -0.125 to 0.125
- merge_proj: bfloat16 [2, 2048, 4096], P(None, 'dp', 'tp'), may hold values from -0.125 to 0.125
- exit_proj: bfloat16 [2, 4096, 4096], P(None, 'dp', 'tp'), may hold values from -0.09375 to 0.09375
- decay_rate: float32 [2, 128, 64], P(None, 'tp'), may hold values from 0.5 to 2
- turn_rate: float32 [2, 128, 64], P(None, 'tp'), may hold values from -3 to 3
- group_step_width: float32 [2, 128], P(None, 'tp'), may hold values from 0.005 to 0.3
- state_in: float32 [2, 2, 128, 64, 16], P(None, None, 'tp'), may hold values from -1 to 1
- state_out: float32 [2, 2, 128, 16, 64], P(None, None, 'tp'), may hold values from -0.5 to 0.5
- skip_gain: float32 [2, 2048], P(None, 'tp'), may hold values from -4 to 4
- carried_state: float32 [2, 2, 128, 8192], P(None, None, 'dp', 'tp'), may hold values from -6 to 6
Outputs:
- updated_tokens: bfloat16 [128, 8, 4096], P('dp', None, 'tp')
- new_state: float32 [2, 2, 128, 8192], P(None, None, 'dp', 'tp')
Inputs may be any that keep to these rules, and one draw needn't show every extreme that they name: `lengths`: each sequence has at least one live slot, and some sequence has all 8.
All inputs are finite; a program needn't handle non-finite values. No bound on the sum of `lengths` on one device may be relied on, other than what follows from the above.
Results may differ from a plain program's by a relative error of at most 0.0055.
Values may be sent and summed in bfloat16 or wider, within the bound.
A program may use at most 128 MiB of HBM per device.

v0:
```python
import functools
import jax
import jax.numpy as jnp
from jax import lax
from jax.experimental import pallas as pl
from jax.experimental.pallas import tpu as pltpu
from jax.sharding import PartitionSpec as P

EPS = 1e-05


def state_update(
    drive, active, current_rate, turn_now, size_now, in_pair, output_couple, skip_now, carried
):
    sequences, positions = active.shape
    groups, entries = current_rate.shape
    members = in_pair.shape[-1]
    real_eig = -current_rate
    step_len = size_now[:, None]
    magnitude = jnp.exp(step_len * real_eig)
    decay_real = magnitude * jnp.cos(step_len * turn_now)
    decay_imag = magnitude * jnp.sin(step_len * turn_now)
    divisor = real_eig * real_eig + turn_now * turn_now
    hold_real = ((decay_real - 1.0) * real_eig + decay_imag * turn_now) / divisor
    hold_imag = (decay_imag * real_eig - (decay_real - 1.0) * turn_now) / divisor
    inject_real = hold_real[..., None] * in_pair[0] - hold_imag[..., None] * in_pair[1]
    inject_imag = hold_real[..., None] * in_pair[1] + hold_imag[..., None] * in_pair[0]
    inputs = drive.reshape(sequences, positions, groups, members)
    pushed_real = jnp.einsum("gpc,bsgc->bsgp", inject_real, inputs, precision=lax.Precision.HIGHEST)
    pushed_imag = jnp.einsum("gpc,bsgc->bsgp", inject_imag, inputs, precision=lax.Precision.HIGHEST)
    state_real_part = carried[0].reshape(sequences, groups, entries)
    state_imaginary = carried[1].reshape(sequences, groups, entries)
    readings = []
    for position in range(positions):
        active_now = (active[:, position] > 0)[:, None, None]
        moved_real = (
            decay_real * state_real_part - decay_imag * state_imaginary + pushed_real[:, position]
        )
        moved_imag = (
            decay_real * state_imaginary + decay_imag * state_real_part + pushed_imag[:, position]
        )
        state_real_part = jnp.where(active_now, moved_real, state_real_part)
        state_imaginary = jnp.where(active_now, moved_imag, state_imaginary)
        readout_value = jnp.einsum(
            "sal,usl->usa", output_couple[0], state_real_part, precision=lax.Precision.HIGHEST
        ) - jnp.einsum(
            "sal,usl->usa", output_couple[1], state_imaginary, precision=lax.Precision.HIGHEST
        )
        readings.append(readout_value)
    readout = jnp.stack(readings, axis=1) + skip_now.reshape(groups, members) * inputs
    final = jnp.stack(
        [
            state_real_part.reshape(sequences, groups * entries),
            state_imaginary.reshape(sequences, groups * entries),
        ]
    )
    return (readout.reshape(sequences * positions, groups * members), final)


def widen_model(values):
    return lax.all_gather(values, "tp", axis=1, tiled=True)


def widen_branch(values):
    return lax.all_gather(values, "tp", axis=1, tiled=True)


def project(gathered, weight):
    return jnp.dot(
        gathered,
        lax.all_gather(weight, "dp", axis=0, tiled=True),
        preferred_element_type=jnp.float32,
    )


def shards(
    tokens,
    lengths,
    norm_gains,
    drive_proj,
    open_proj,
    glu_proj,
    merge_proj,
    exit_proj,
    decay_rate,
    turn_rate,
    group_step_width,
    state_in,
    state_out,
    skip_gain,
    carried_state,
):
    sequences, positions, local_width = tokens.shape
    row_count = sequences * positions
    model_width = local_width * lax.axis_size("tp")
    first_col = lax.axis_index("tp") * local_width
    active = (lax.broadcasted_iota(jnp.int32, (sequences, positions), 1) < lengths[:, None]).astype(
        jnp.int32
    )
    active_rows = active.reshape(row_count, 1).astype(jnp.float32)
    residual = tokens.reshape(row_count, local_width)
    states = []
    for layer_index in range(norm_gains.shape[0]):
        norm_gain = norm_gains[layer_index]
        own_values = residual.astype(jnp.float32)
        squared_sum = lax.psum(jnp.sum(own_values * own_values, axis=1), "tp")
        inverse_rms = lax.rsqrt(squared_sum / model_width + EPS)[:, None]
        own_gain = lax.dynamic_slice_in_dim(norm_gain, first_col, local_width, 0)
        gathered = widen_model((own_values * inverse_rms * own_gain).astype(jnp.bfloat16))
        drive = project(gathered, drive_proj[layer_index])
        gate_open = jax.nn.sigmoid(project(gathered, open_proj[layer_index]))
        readout, final = state_update(
            drive,
            active,
            decay_rate[layer_index],
            turn_rate[layer_index],
            group_step_width[layer_index],
            state_in[layer_index],
            state_out[layer_index],
            skip_gain[layer_index],
            carried_state[layer_index],
        )
        states.append(final)
        activated = jax.nn.gelu(readout).astype(jnp.bfloat16)
        gating = project(widen_branch(activated), glu_proj[layer_index])
        gated = (activated.astype(jnp.float32) * jax.nn.sigmoid(gating)).astype(jnp.bfloat16)
        merged = project(widen_branch(gated), merge_proj[layer_index])
        mixed = (gate_open * merged).astype(jnp.bfloat16)
        branch = project(widen_model(mixed), exit_proj[layer_index])
        residual = (residual.astype(jnp.float32) + active_rows * branch).astype(jnp.bfloat16)
    return (residual.reshape(sequences, positions, local_width), jnp.stack(states))


def fused_kernel(
    dims,
    tok, lens, gains, decay, inject, outmix, skip, carried,
    w_drive, w_open, w_glu, w_merge, w_exit,
    out_tok, out_state,
    v_drive, v_open, v_glu, v_merge, v_exit,
    row_send, row_recv, a_send, a_recv, c_send, c_recv,
    x_src, x_recv, y_src, y_recv, st_recv, st_new, nst_recv, fin_recv,
    inv_buf, gate_buf, act_buf, len_recv, pack_own, unpack,
    w_sem, row_ss, row_rs, a_ss, a_rs, c_ss, c_rs, x_ss, x_rs, y_ss, y_rs,
    st_ss, st_rs, n_ss, n_rs, f_ss, f_rs, l_ss, l_rs,
):
    layers, nd, nt, all_rows, model, lots = dims
    ratio = nt // nd
    rows = all_rows // lots
    chunk = rows // nd
    half = rows // 2
    f32, bf16 = jnp.float32, jnp.bfloat16
    d = lax.axis_index("dp")
    t = lax.axis_index("tp")
    home = t // ratio
    place = lax.rem(t, ratio)
    batch_own = carried.shape[2]
    batch = batch_own * nd
    own_ch = inject.shape[3] // 2
    width = c_send.shape[-1] // 2
    steps = tok.shape[0] // batch_own

    loads = []
    for i, (src, dst) in enumerate(
        ((w_drive, v_drive), (w_open, v_open), (w_glu, v_glu), (w_merge, v_merge), (w_exit, v_exit))
    ):
        for l in range(layers):
            copy = pltpu.make_async_copy(src.at[l], dst.at[l], w_sem.at[i, l])
            copy.start()
            loads.append(copy)

    def weight(i, l):
        loads[i * layers + l].wait()

    barrier = pltpu.get_barrier_semaphore()
    total = nd * nt
    flat = t * nd + d

    def greet(i, carry):
        other = lax.rem(flat + i, total)
        pl.semaphore_signal(
            barrier, inc=1,
            device_id={"tp": other // nd, "dp": lax.rem(other, nd)},
            device_id_type=pl.DeviceIdType.MESH,
        )
        return carry

    lax.fori_loop(1, total, greet, 0)
    pl.semaphore_wait(barrier, total - 1)

    pending = []

    def send(src, dst, ss, rs, to_dp, to_tp, is_self):
        far = pltpu.make_async_remote_copy(
            src_ref=src, dst_ref=dst, send_sem=ss, recv_sem=rs,
            device_id={"tp": to_tp, "dp": to_dp}, device_id_type=pl.DeviceIdType.MESH,
        )
        if is_self is None:
            far.start()
        else:
            @pl.when(is_self)
            def _():
                pltpu.make_async_copy(src, dst, rs).start()

            @pl.when(jnp.logical_not(is_self))
            def _():
                far.start()

        pending.append((far, is_self))

    def arrive(dst, rs):
        pltpu.make_async_copy(dst, dst, rs).wait()

    def send_row(k, c):
        send(row_send.at[k, c], row_recv.at[k, d], row_ss.at[k, c], row_rs.at[k, d], c, t, d == c)

    def row_sum(k):
        acc = None
        for s in range(nd):
            arrive(row_recv.at[k, s], row_rs.at[k, s])
            v = row_recv[k, s].astype(f32)
            acc = v if acc is None else acc + v
        return acc

    def spread_x(k):
        slot = place * nd + d
        for j in range(nd):
            to = lax.rem(home + j, nd) * ratio + place
            send(
                x_src.at[k], x_recv.at[k, place, pl.ds(d * chunk, chunk)],
                x_ss.at[k, j], x_rs.at[k, slot], home, to, (d == home) if j == 0 else None,
            )

    def forward_x(k):
        for s in range(nd):
            piece = x_recv.at[k, place, pl.ds(s * chunk, chunk)]
            arrive(piece, x_rs.at[k, place * nd + s])
            for i in range(1, ratio):
                to = home * ratio + lax.rem(place + i, ratio)
                send(
                    piece, piece, x_ss.at[k, nd + s * (ratio - 1) + i - 1],
                    x_rs.at[k, place * nd + s], d, to, None,
                )

    def take_x(k):
        for i in range(1, ratio):
            p = lax.rem(place + i, ratio)
            for s in range(nd):
                arrive(x_recv.at[k, p, pl.ds(s * chunk, chunk)], x_rs.at[k, p * nd + s])

    def spread_y(k):
        slot = place * nd + d
        for j in range(nd):
            to = lax.rem(home + j, nd) * ratio + place
            send(
                y_src.at[k], y_recv.at[k, slot],
                y_ss.at[k, j], y_rs.at[k, slot], home, to, (d == home) if j == 0 else None,
            )

    def forward_y(k):
        for s in range(nd):
            slot = place * nd + s
            piece = y_recv.at[k, slot]
            arrive(piece, y_rs.at[k, slot])
            for i in range(1, ratio):
                to = home * ratio + lax.rem(place + i, ratio)
                send(
                    piece, piece, y_ss.at[k, nd + s * (ratio - 1) + i - 1],
                    y_rs.at[k, slot], d, to, None,
                )

    def take_y(k):
        for i in range(1, ratio):
            p = lax.rem(place + i, ratio)
            for s in range(nd):
                arrive(y_recv.at[k, p * nd + s], y_rs.at[k, p * nd + s])
        parts = []
        for p in range(ratio):
            for s in range(nd):
                v = y_recv[k, p * nd + s]
                parts.append(jnp.concatenate([v[:, :width], v[:, width:]], axis=0))
        return jnp.concatenate(parts, axis=1)

    def fold(v):
        return jnp.concatenate([v[:half], v[half:]], axis=1)

    for c in range(nd):
        send(lens, len_recv.at[d], l_ss.at[c], l_rs.at[d], c, t, d == c)
    len_row = None
    for s in range(nd):
        arrive(len_recv.at[s], l_rs.at[s])
        len_row = len_recv[s] if len_row is None else len_row + len_recv[s]
    down = lax.broadcasted_iota(jnp.int32, (batch, batch), 0)
    along = lax.broadcasted_iota(jnp.int32, (batch, batch), 1)
    before = jnp.where(down < along, 1.0, 0.0).astype(bf16)
    start_row = jnp.dot(len_row.astype(bf16), before, preferred_element_type=f32)

    def upright(v):
        wide = jnp.broadcast_to(v[0:1], (batch, batch))
        return jnp.sum(jnp.where(down == along, wide, 0.0), axis=1, keepdims=True)

    len_col, start_col = upright(len_row), upright(start_row)
    count = lax.broadcasted_iota(jnp.int32, (batch, all_rows), 1).astype(f32)
    for step in range(steps):
        hit = jnp.logical_and(count == start_col + step, len_col > step)
        unpack[step * batch:(step + 1) * batch, :] = jnp.where(hit, 1.0, 0.0).astype(bf16)
    own_rows = tok.shape[0]
    local = lax.broadcasted_iota(jnp.int32, (batch, own_rows), 0) - d * batch_own
    item = lax.broadcasted_iota(jnp.int32, (batch, own_rows), 1)
    inside = jnp.logical_and(item >= local * steps, item < (local + 1) * steps)
    expand = jnp.where(inside, 1.0, 0.0)
    order = (lax.broadcasted_iota(jnp.int32, len_row.shape, 1) - d * batch_own).astype(f32)
    exact = functools.partial(
        jnp.dot, preferred_element_type=f32, precision=lax.Precision.HIGHEST
    )
    spot = exact(start_row - steps * order, expand)[0:1]
    spot = spot + lax.broadcasted_iota(jnp.int32, (1, own_rows), 1).astype(f32)
    end = exact(start_row + len_row, expand)[0:1]
    spot = jnp.where(spot < end, spot, -1.0)
    tall = lax.broadcasted_iota(jnp.int32, (all_rows, own_rows), 0).astype(f32)
    pack_own[...] = jnp.where(tall == spot, 1.0, 0.0).astype(bf16)

    def turned(a, b):
        return lax.dot_general(a, b, (((0,), (0,)), ((), ())), preferred_element_type=f32)

    every = range(lots)
    for h in every:
        for c in range(nd):
            top = h * rows + c * chunk
            part = jnp.dot(pack_own[top:top + chunk, :], tok[...], preferred_element_type=f32)
            row_send[h, c] = part.astype(bf16)
            send_row(h, c)
    for c in range(nd):
        send(
            carried.at[:, :, :, pl.ds(c * own_ch, own_ch)], st_recv.at[d],
            st_ss.at[c], st_rs.at[d], c, t, d == c,
        )
    cols = tok.shape[1]
    residual = []
    for h in every:
        residual.append(row_sum(h).astype(bf16))
        x_src[h] = residual[h]
        spread_x(h)
    for s in range(nd):
        arrive(st_recv.at[s], st_rs.at[s])
    for l in range(layers):
        first, second = 2 * l * lots, (2 * l + 1) * lots
        k_open = (1 + 3 * l) * lots
        k_merge, k_exit = k_open + lots, k_open + 2 * lots
        for h in every:
            forward_x(first + h)
        weight(0, l)
        normed = []
        for h in every:
            take_x(first + h)
            scaled, squares = [], None
            for p in range(ratio):
                raw = x_recv[first + h, p].astype(f32)
                sq = jnp.sum(raw * raw, axis=1, keepdims=True)
                squares = sq if squares is None else squares + sq
                scaled.append((raw * gains[l, d, p]).astype(bf16))
            normed.append(jnp.concatenate(scaled, axis=1))
            drive = jnp.dot(normed[h], v_drive[l], preferred_element_type=f32)
            high = squares.astype(bf16)
            low = (squares - high.astype(f32)).astype(bf16)
            lane = lax.broadcasted_iota(jnp.int32, (rows, width), 1)
            tail = jnp.where(
                lane == 0, high.astype(f32), jnp.where(lane == 1, low.astype(f32), 0.0)
            ).astype(bf16)
            k = l * lots + h
            for c in range(nd):
                a_send[k, c] = jnp.concatenate(
                    [drive[:, c * width:(c + 1) * width].astype(bf16), tail], axis=1
                )
                send(a_send.at[k, c], a_recv.at[k, d], a_ss.at[k, c], a_rs.at[k, d], c, t, d == c)
        weight(1, l)
        for h in every:
            for c in range(nd):
                part = jnp.dot(
                    normed[h][c * chunk:(c + 1) * chunk], v_open[l], preferred_element_type=f32
                )
                row_send[k_open + h, c] = part.astype(bf16)
                send_row(k_open + h, c)
        feeds = []
        for h in every:
            k = l * lots + h
            summed = None
            for s in range(nd):
                arrive(a_recv.at[k, s], a_rs.at[k, s])
                v = a_recv[k, s].astype(f32)
                summed = v if summed is None else summed + v
            full_sq = summed[:, width:width + 1] + summed[:, width + 1:width + 2]
            inverse = lax.rsqrt(full_sq / model + EPS)
            inv_buf[h * rows:(h + 1) * rows, :] = jnp.broadcast_to(inverse, (rows, 128))
            lane2 = lax.broadcasted_iota(jnp.int32, summed.shape, 1)
            feed = jnp.where(lane2 < width, summed * inverse, jnp.where(lane2 == width, 1.0, 0.0))
            feeds.append(feed.astype(bf16))
        feed = jnp.concatenate(feeds, axis=0)
        real = jnp.concatenate([st_recv[s, l, 0] for s in range(nd)], axis=0)
        imag = jnp.concatenate([st_recv[s, l, 1] for s in range(nd)], axis=0)
        dr, di = decay[l, 0, d], decay[l, 1, d]
        for step in range(steps):
            span = slice(step * batch, (step + 1) * batch)
            u = jnp.dot(unpack[span, :], feed, preferred_element_type=f32)
            live = u[:, width:width + 1] > 0.5
            push = jnp.dot(u.astype(bf16), inject[l, d], preferred_element_type=f32)
            moved_real = dr * real - di * imag + push[:, :own_ch]
            moved_imag = dr * imag + di * real + push[:, own_ch:]
            real = jnp.where(live, moved_real, real)
            imag = jnp.where(live, moved_imag, imag)
            both = jnp.concatenate([real, imag], axis=1).astype(bf16)
            read = jnp.dot(both, outmix[l, d], preferred_element_type=f32) + skip[l, d] * u
            act_buf[span, :] = jax.nn.gelu(read).astype(bf16)
        st_new[l, 0] = real
        st_new[l, 1] = imag
        packed_all = turned(unpack[...], act_buf[...]).astype(bf16)
        activated = []
        for h in every:
            packed = packed_all[h * rows:(h + 1) * rows]
            activated.append(fold(packed[:, :width]))
            y_src[first + h] = activated[h]
            spread_y(first + h)
        for h in every:
            mine = pl.ds(pl.multiple_of(h * rows + d * chunk, chunk), chunk)
            gate_buf[h] = jax.nn.sigmoid(row_sum(k_open + h) * inv_buf[mine, 0:1])
        weight(2, l)
        for h in every:
            forward_y(first + h)
        for h in every:
            wide = take_y(first + h)
            gating = jnp.dot(wide, v_glu[l], preferred_element_type=f32).astype(bf16)
            k = l * lots + h
            for c in range(nd):
                c_send[k, c] = fold(gating[:, c * width:(c + 1) * width])
                send(c_send.at[k, c], c_recv.at[k, d], c_ss.at[k, c], c_rs.at[k, d], c, t, d == c)
        for h in every:
            k = l * lots + h
            summed = None
            for s in range(nd):
                arrive(c_recv.at[k, s], c_rs.at[k, s])
                v = c_recv[k, s].astype(f32)
                summed = v if summed is None else summed + v
            gated = activated[h].astype(f32) * jax.nn.sigmoid(summed)
            y_src[second + h] = gated.astype(bf16)
            spread_y(second + h)
        weight(3, l)
        for h in every:
            forward_y(second + h)
        for h in every:
            wide = take_y(second + h)
            for c in range(nd):
                part = jnp.dot(
                    wide[c * chunk:(c + 1) * chunk], v_merge[l], preferred_element_type=f32
                )
                row_send[k_merge + h, c] = part.astype(bf16)
                send_row(k_merge + h, c)
        for h in every:
            x_src[second + h] = (gate_buf[h] * row_sum(k_merge + h)).astype(bf16)
            spread_x(second + h)
        for c in range(nd):
            send(
                st_new.at[l, :, pl.ds(c * batch_own, batch_own)], nst_recv.at[d, l],
                n_ss.at[l, c], n_rs.at[l, d], c, t, d == c,
            )
        weight(4, l)
        for h in every:
            forward_x(second + h)
        for h in every:
            take_x(second + h)
            for c in range(nd):
                part = None
                for p in range(ratio):
                    v = jnp.dot(
                        x_recv[second + h, p, c * chunk:(c + 1) * chunk],
                        v_exit[l, p * cols:(p + 1) * cols],
                        preferred_element_type=f32,
                    )
                    part = v if part is None else part + v
                row_send[k_exit + h, c] = part.astype(bf16)
                send_row(k_exit + h, c)
        for h in every:
            residual[h] = (residual[h].astype(f32) + row_sum(k_exit + h)).astype(bf16)
            k = (2 * l + 2) * lots + h
            x_src[k] = residual[h]
            if l + 1 < layers:
                spread_x(k)
            else:
                for c in range(nd):
                    send(
                        x_src.at[k], fin_recv.at[pl.ds(h * rows + d * chunk, chunk)],
                        f_ss.at[h, c], f_rs.at[h, d], c, t, d == c,
                    )
    for l in range(layers):
        for s in range(nd):
            arrive(nst_recv.at[s, l], n_rs.at[l, s])
            for part in range(2):
                out_state[l, part, :, s * own_ch:(s + 1) * own_ch] = nst_recv[s, l, part]
    for h in every:
        for s in range(nd):
            arrive(fin_recv.at[pl.ds(h * rows + s * chunk, chunk)], f_rs.at[h, s])
    spread = turned(pack_own[...], fin_recv[...])
    keep = turned(pack_own[...], jnp.ones((all_rows, 128), bf16))[:, 0:1]
    out_tok[...] = jnp.where(keep > 0.5, spread, tok[...].astype(f32)).astype(bf16)
    for far, is_self in pending:
        if is_self is None:
            far.wait_send()
        else:
            pl.when(jnp.logical_not(is_self))(far.wait_send)


def fused_shards(
    tokens, lengths, norm_gains, drive_proj, open_proj, glu_proj, merge_proj, exit_proj,
    decay_rate, turn_rate, group_step_width, state_in, state_out, skip_gain, carried_state,
):
    f32, bf16 = jnp.float32, jnp.bfloat16
    nd, nt = lax.axis_size("dp"), lax.axis_size("tp")
    d, t = lax.axis_index("dp"), lax.axis_index("tp")
    layers = norm_gains.shape[0]
    own, steps, cols = tokens.shape
    batch = own * nd
    rows = 3 * batch
    model = cols * nt
    ratio = nt // nd
    groups_own = decay_rate.shape[1]
    few = groups_own // nd
    entries = decay_rate.shape[2]
    members = state_in.shape[-1]
    width = few * members
    own_ch = few * entries
    chunk = rows // nd

    place = jnp.arange(batch, dtype=jnp.int32) // own
    lens = jnp.where(place == d, jnp.tile(lengths, nd), 0).astype(f32)
    lens = jnp.broadcast_to(lens[None, :], (8, batch))
    gains = norm_gains.reshape(layers, nd, ratio, 1, cols)

    real_eig = -decay_rate
    turn_now = turn_rate
    step_len = group_step_width[..., None]
    in_pair, out_pair = state_in, state_out
    skip_now = skip_gain.reshape(layers, nd, 1, width)
    magnitude = jnp.exp(step_len * real_eig)
    decay_real = magnitude * jnp.cos(step_len * turn_now)
    decay_imag = magnitude * jnp.sin(step_len * turn_now)
    divisor = real_eig * real_eig + turn_now * turn_now
    hold_real = ((decay_real - 1.0) * real_eig + decay_imag * turn_now) / divisor
    hold_imag = (decay_imag * real_eig - (decay_real - 1.0) * turn_now) / divisor
    inject_real = hold_real[..., None] * in_pair[:, 0] - hold_imag[..., None] * in_pair[:, 1]
    inject_imag = hold_real[..., None] * in_pair[:, 1] + hold_imag[..., None] * in_pair[:, 0]
    eye = jnp.eye(few, dtype=f32)
    both = jnp.stack([inject_real, inject_imag], axis=1).reshape(
        layers, 2, nd, few, entries, members
    )
    inject = (
        jnp.transpose(both, (0, 2, 3, 5, 1, 4))[:, :, :, :, :, None, :]
        * eye[None, None, :, None, None, :, None]
    ).reshape(layers, nd, width, 2 * own_ch)
    inject = jnp.pad(inject, ((0, 0), (0, 0), (0, width), (0, 0))).astype(bf16)
    signed = jnp.stack([out_pair[:, 0], -out_pair[:, 1]], axis=1).reshape(
        layers, 2, nd, few, members, entries
    )
    outmix = (
        jnp.transpose(signed, (0, 2, 1, 3, 5, 4))[:, :, :, :, :, None, :]
        * eye[None, None, None, :, None, :, None]
    ).reshape(layers, nd, 2 * own_ch, width)
    outmix = jnp.pad(outmix, ((0, 0), (0, 0), (0, 0), (0, width))).astype(bf16)
    skip = jnp.pad(skip_now, ((0, 0), (0, 0), (0, 0), (0, width)))
    decay = jnp.stack([decay_real, decay_imag], axis=1).reshape(layers, 2, nd, 1, own_ch)

    lots = 3
    n_row = (1 + 3 * layers) * lots
    n_col = layers * lots
    n_all = 2 * layers * lots
    lot = rows // lots
    piece = chunk // lots
    half = lot // 2
    vm = pltpu.VMEM
    dma = pltpu.SemaphoreType.DMA
    weights = (drive_proj, open_proj, glu_proj, merge_proj, exit_proj)
    scratch = [vm(w.shape, bf16) for w in weights] + [
        vm((n_row, nd, piece, cols), bf16),
        vm((n_row, nd, piece, cols), bf16),
        vm((n_col, nd, lot, 2 * width), bf16),
        vm((n_col, nd, lot, 2 * width), bf16),
        vm((n_col, nd, half, 2 * width), bf16),
        vm((n_col, nd, half, 2 * width), bf16),
        vm((n_all + lots, piece, cols), bf16),
        vm((n_all, ratio, lot, cols), bf16),
        vm((n_all, half, 2 * width), bf16),
        vm((n_all, nt, half, 2 * width), bf16),
        vm((nd, layers, 2, own, own_ch), f32),
        vm((layers, 2, batch, own_ch), f32),
        vm((nd, layers, 2, own, own_ch), f32),
        vm((rows, cols), bf16),
        vm((rows, 128), f32),
        vm((lots, piece, cols), f32),
        vm((steps * batch, 2 * width), bf16),
        vm((nd, 8, batch), f32),
        vm((rows, own * steps), bf16),
        vm((steps * batch, rows), bf16),
        dma((5, layers)),
        dma((n_row, nd)), dma((n_row, nd)),
        dma((n_col, nd)), dma((n_col, nd)),
        dma((n_col, nd)), dma((n_col, nd)),
        dma((n_all, nd * ratio)), dma((n_all, nt)),
        dma((n_all, nd * ratio)), dma((n_all, nt)),
        dma((nd,)), dma((nd,)),
        dma((layers, nd)), dma((layers, nd)),
        dma((lots, nd)), dma((lots, nd)),
        dma((nd,)), dma((nd,)),
    ]
    inside = pl.BlockSpec(memory_space=pltpu.VMEM)
    outside = pl.BlockSpec(memory_space=pl.ANY)
    out_rows, out_state = pl.pallas_call(
        functools.partial(fused_kernel, (layers, nd, nt, rows, model, lots)),
        out_shape=(
            jax.ShapeDtypeStruct((own * steps, cols), bf16),
            jax.ShapeDtypeStruct(carried_state.shape, f32),
        ),
        in_specs=[inside] * 8 + [outside] * 5,
        out_specs=(inside, inside),
        scratch_shapes=scratch,
        compiler_params=pltpu.CompilerParams(
            collective_id=0, has_side_effects=True, vmem_limit_bytes=60 * 1024 * 1024
        ),
    )(
        tokens.reshape(own * steps, cols), lens,
        gains, decay, inject, outmix, skip, carried_state, *weights,
    )
    return out_rows.reshape(own, steps, cols), out_state


def solution(mesh):
    in_specs = (
        P("dp", None, "tp"),
        P("dp"),
        P(),
        P(None, "dp", "tp"),
        P(None, "dp", "tp"),
        P(None, "dp", "tp"),
        P(None, "dp", "tp"),
        P(None, "dp", "tp"),
        P(None, "tp", None),
        P(None, "tp", None),
        P(None, "tp"),
        P(None, None, "tp", None, None),
        P(None, None, "tp", None, None),
        P(None, "tp"),
        P(None, None, "dp", "tp"),
    )
    out_specs = (P("dp", None, "tp"), P(None, None, "dp", "tp"))
    ways, nd = mesh.shape["tp"], mesh.shape["dp"]

    def run(*args):
        groups = args[8].shape[1] // ways
        whole_groups = groups % nd == 0 and ways % nd == 0
        body = fused_shards if whole_groups else shards
        return jax.shard_map(body, mesh=mesh, in_specs=in_specs, out_specs=out_specs, check_vma=False)(*args)

    return run
```

profile of v0, /device:TPU:0, one launch (start us, length us, event | category | flops | bytes accessed | tf_op | source)
XLA Modules:
  0.0 173.9 jit_solution(18048396597921281513)
XLA Ops:
  0.7 0.1 copy.20
  0.7 0.7 tile.4
  1.4 0.1 tile.10
  1.5 0.6 broadcast_in_dim.4.lens
  2.1 0.8 reshape.77
  2.9 0.6 pad.16.skip
  3.5 1.4 reshape.76.gains
  4.9 0.9 add_divide_fusion
  5.8 0.1 stack.26
  5.9 0.1 stack.27
  6.0 0.6 pad_maximum_fusion.decay
  6.6 0.1 mul.139
  6.7 0.2 mul.140
  6.9 0.0 copy-start.2
  6.9 0.1 copy.22
  7.0 0.1 mul.133
  7.1 0.2 mul.134
  7.3 0.1 multiply_subtract_fusion
  7.4 1.2 copy.19
  8.7 0.2 copy.21
  8.9 0.5 mul.137
  9.4 1.4 mul.138
  10.7 0.6 copy.23
  11.4 0.2 multiply_convert_fusion
  11.6 1.2 pad.15.outmix
  12.8 0.4 mul.131
  13.2 1.3 mul.132
  14.5 0.1 multiply_convert_fusion.1
  14.7 1.1 pad.14.inject
  15.7 154.6 %shard_map.158 = (bf16[256,512]{1,0:T(8,128)(2,1)}, f32[2,2,32,1024]{3,2,1,0:T(8,128)}) custom-call(bf16[256,512]{1,0:T(8,128)(2,1)} %bitcast.18, f32[8,128]{1,0:T(8,128)} %broadcast_in_dim.4.lens, f32[2,4,2,1,512]{4,3,2,1,0:T(1,128)} %reshape.76.gains, f32[2,2,4,1,256]{4,3,2,1,0:T(1,128)} %pad_maximum_fusion.decay, bf16[2,4,128,512]{3,2,1,0:T(8,128)(2,1)} %pad.14.inject, ...), custom_call_target="tpu_custom_call" | custom-call | tf_op jit(solution)/shard_map/pallas_call | solution.py:613
  170.4 1.7 copy.26
  172.0 1.9 %copy.27 = f32[2,2,32,1024]{3,2,1,0:T(8,128)} copy(f32[2,2,32,1024]{3,2,1,0:T(8,128)} %get-tuple-element.17) | data formatting | bytes 1048576
  (10 shorter events, 0.1 us)
Async XLA Ops:
  0.6 6.6 %copy-start.1 = (f32[2,2,16,64,16]{3,4,2,1,0:T(8,128)S(1)}, f32[2,2,16,64,16]{3,4,2,1,0:T(8,128)}, u32[]{:S(2)}) copy-start(f32[2,2,16,64,16]{3,4,2,1,0:T(8,128)} %param.26) | copy-start | bytes 786436
  6.9 1.8 %copy-start.2 = (f32[2,2,16,16,64]{4,3,2,1,0:T(8,128)S(1)}, f32[2,2,16,16,64]{4,3,2,1,0:T(8,128)}, u32[]{:S(2)}) copy-start(f32[2,2,16,16,64]{4,3,2,1,0:T(8,128)} %param.27) | copy-start | bytes 786436
  11.4 1.4 copy-start
where the time goes:
time: 174 us
  Pallas kernels  155 us (89%)
  local copies, waits for them, and re-layouts  16.5 us (9%)
  other arithmetic  2.02 us (1%)
    pallas_call x1, Pallas kernels, fused_shards(): pl.pallas_call(functools.partial(fused_kernel, (layers, nd, nt, rows, mod...  155 us
    unnamed x8, local copies, waits for them, and re-layouts  3.57 us

commit v1 on v0

--- a/solution.py
+++ b/solution.py
@@ -131,16 +131,21 @@
     return (residual.reshape(sequences, positions, local_width), jnp.stack(states))
 
 
+LOTS = 3
+SKEW = 0
+
+
 def fused_kernel(
     dims,
-    tok, lens, gains, decay, inject, outmix, skip, carried,
+    tok, lens, gains, rate, turn, size, s_in, s_out, skip, carried,
     w_drive, w_open, w_glu, w_merge, w_exit,
     out_tok, out_state,
-    v_drive, v_open, v_glu, v_merge, v_exit,
+    v_drive, v_open, v_glu, v_merge, v_exit, v_tok, v_in, v_out,
+    par, inj, omx, len_own,
     row_send, row_recv, a_send, a_recv, c_send, c_recv,
-    x_src, x_recv, y_src, y_recv, st_recv, st_new, nst_recv, fin_recv,
-    inv_buf, gate_buf, act_buf, len_recv, pack_own, unpack,
-    w_sem, row_ss, row_rs, a_ss, a_rs, c_ss, c_rs, x_ss, x_rs, y_ss, y_rs,
+    x_src, x_recv, y_src, y_recv, st_recv, st_new, fin_recv,
+    norm_buf, inv_buf, act_buf, feed_buf, len_recv, pack_own, unpack,
+    w_sem, in_sem, row_ss, row_rs, a_ss, a_rs, c_ss, c_rs, x_ss, x_rs, y_ss, y_rs,
     st_ss, st_rs, n_ss, n_rs, f_ss, f_rs, l_ss, l_rs,
 ):
     layers, nd, nt, all_rows, model, lots = dims
@@ -155,21 +160,21 @@
     place = lax.rem(t, ratio)
     batch_own = carried.shape[2]
     batch = batch_own * nd
-    own_ch = inject.shape[3] // 2
-    width = c_send.shape[-1] // 2
-    steps = tok.shape[0] // batch_own
-
-    loads = []
-    for i, (src, dst) in enumerate(
-        ((w_drive, v_drive), (w_open, v_open), (w_glu, v_glu), (w_merge, v_merge), (w_exit, v_exit))
-    ):
-        for l in range(layers):
-            copy = pltpu.make_async_copy(src.at[l], dst.at[l], w_sem.at[i, l])
-            copy.start()
-            loads.append(copy)
-
-    def weight(i, l):
-        loads[i * layers + l].wait()
+    few, members, entries = v_in.shape[2:]
+    own_ch = few * entries
+    width = few * members
+    own_rows = v_tok.shape[0]
+    steps = own_rows // batch_own
+    cols = v_tok.shape[1]
+
+    def load(src, dst, sem):
+        copy = pltpu.make_async_copy(src, dst, sem)
+        copy.start()
+        return copy
+
+    tok_load = load(tok, v_tok, in_sem.at[0])
+    in_load = load(s_in.at[:, :, pl.ds(d * few, few)], v_in, in_sem.at[1])
+    out_load = load(s_out.at[:, :, pl.ds(d * few, few)], v_out, in_sem.at[2])
 
     barrier = pltpu.get_barrier_semaphore()
     total = nd * nt
@@ -185,7 +190,17 @@
         return carry
 
     lax.fori_loop(1, total, greet, 0)
-    pl.semaphore_wait(barrier, total - 1)
+
+    loads = {}
+    for l in range(layers):
+        for i, (src, dst) in enumerate(
+            ((w_drive, v_drive), (w_open, v_open), (w_glu, v_glu), (w_merge, v_merge), (w_exit, v_exit))
+        ):
+            loads[i, l] = load(src.at[l], dst.at[l], w_sem.at[i, l])
+
+    def weight(i, l):
+        if (i, l) in loads:
+            loads.pop((i, l)).wait()
 
     pending = []
 
@@ -221,6 +236,12 @@
             acc = v if acc is None else acc + v
         return acc
 
+    def send_rows(k, part):
+        part = part.astype(bf16)
+        for c in range(nd):
+            row_send[k, c] = part[c * chunk:(c + 1) * chunk]
+            send_row(k, c)
+
     def spread_x(k):
         slot = place * nd + d
         for j in range(nd):
@@ -283,8 +304,76 @@
     def fold(v):
         return jnp.concatenate([v[:half], v[half:]], axis=1)
 
+    def send_states(l):
+        for c in range(nd):
+            send(
+                carried.at[l, :, :, pl.ds(c * own_ch, own_ch)], st_recv.at[l, d],
+                st_ss.at[l, c], st_rs.at[l, d], c, t, d == c,
+            )
+
+    def return_states(l):
+        for c in range(nd):
+            send(
+                st_new.at[l, :, pl.ds(c * batch_own, batch_own)],
+                out_state.at[l, :, :, pl.ds(pl.multiple_of(d * own_ch, own_ch), own_ch)],
+                n_ss.at[l, c], n_rs.at[l, d], c, t, d == c,
+            )
+
+    wide = jnp.concatenate([lens[...].astype(f32)] * nd, axis=1)
+    owner = lax.broadcasted_iota(jnp.int32, wide.shape, 1) // batch_own
+    len_own[...] = jnp.broadcast_to(jnp.where(owner == d, wide, 0.0), len_own.shape)
+
+    def upright_of(v, n):
+        a = lax.broadcasted_iota(jnp.int32, (n, n), 0)
+        b = lax.broadcasted_iota(jnp.int32, (n, n), 1)
+        return jnp.sum(jnp.where(a == b, jnp.broadcast_to(v, (n, n)), 0.0), axis=1, keepdims=True)
+
+    for l in range(layers):
+        real_eig, turn_now = -rate[l], turn[l]
+        step_len = upright_of(size[l:l + 1, :], size.shape[1])
+        magnitude = jnp.exp(step_len * real_eig)
+        decay_real = magnitude * jnp.cos(step_len * turn_now)
+        decay_imag = magnitude * jnp.sin(step_len * turn_now)
+        divisor = real_eig * real_eig + turn_now * turn_now
+        par[l, 0] = decay_real
+        par[l, 1] = decay_imag
+        par[l, 2] = ((decay_real - 1.0) * real_eig + decay_imag * turn_now) / divisor
+        par[l, 3] = (decay_imag * real_eig - (decay_real - 1.0) * turn_now) / divisor
+
+    pl.semaphore_wait(barrier, total - 1)
     for c in range(nd):
-        send(lens, len_recv.at[d], l_ss.at[c], l_rs.at[d], c, t, d == c)
+        send(len_own, len_recv.at[d], l_ss.at[c], l_rs.at[d], c, t, d == c)
+
+    in_load.wait()
+    out_load.wait()
+
+    def blocks(j, a, b):
+        blank = jnp.zeros((members, entries), f32)
+        row = [blank] * j + [a] + [blank] * (few - 1 - j) + [blank] * j + [b] + [blank] * (few - 1 - j)
+        return jnp.concatenate(row, axis=1).astype(bf16)
+
+    for l in range(layers):
+        for j in range(few):
+            hold_real = par[l, 2, pl.ds(d * few + j, 1), :]
+            hold_imag = par[l, 3, pl.ds(d * few + j, 1), :]
+            a, b = v_in[l, 0, j], v_in[l, 1, j]
+            inj[l, j * members:(j + 1) * members, :] = blocks(
+                j, hold_real * a - hold_imag * b, hold_real * b + hold_imag * a
+            )
+            omx[l, j * members:(j + 1) * members, :] = blocks(j, v_out[l, 0, j], -v_out[l, 1, j])
+        inj[l, width:, :] = jnp.zeros((width, 2 * own_ch), bf16)
+        omx[l, width:, :] = jnp.zeros((width, 2 * own_ch), bf16)
+
+    def decays(l, part):
+        return jnp.concatenate([par[l, part, pl.ds(d * few + j, 1), :] for j in range(few)], axis=1)
+
+    def skips(l):
+        own = None
+        for s in range(nd):
+            v = skip[l:l + 1, s * width:(s + 1) * width]
+            own = v if own is None else jnp.where(d == s, v, own)
+        return jnp.concatenate([own, jnp.zeros_like(own)], axis=1)
+
     len_row = None
     for s in range(nd):
         arrive(len_recv.at[s], l_rs.at[s])
@@ -294,16 +383,6 @@
     before = jnp.where(down < along, 1.0, 0.0).astype(bf16)
     start_row = jnp.dot(len_row.astype(bf16), before, preferred_element_type=f32)
 
-    def upright(v):
-        wide = jnp.broadcast_to(v[0:1], (batch, batch))
-        return jnp.sum(jnp.where(down == along, wide, 0.0), axis=1, keepdims=True)
-
-    len_col, start_col = upright(len_row), upright(start_row)
-    count = lax.broadcasted_iota(jnp.int32, (batch, all_rows), 1).astype(f32)
-    for step in range(steps):
-        hit = jnp.logical_and(count == start_col + step, len_col > step)
-        unpack[step * batch:(step + 1) * batch, :] = jnp.where(hit, 1.0, 0.0).astype(bf16)
-    own_rows = tok.shape[0]
     local = lax.broadcasted_iota(jnp.int32, (batch, own_rows), 0) - d * batch_own
     item = lax.broadcasted_iota(jnp.int32, (batch, own_rows), 1)
     inside = jnp.logical_and(item >= local * steps, item < (local + 1) * steps)
@@ -323,64 +402,58 @@
         return lax.dot_general(a, b, (((0,), (0,)), ((), ())), preferred_element_type=f32)
 
     every = range(lots)
+    tok_load.wait()
     for h in every:
+        send_rows(h, jnp.dot(
+            pack_own[h * rows:(h + 1) * rows, :], v_tok[...], preferred_element_type=f32
+        ))
+
+    len_col, start_col = upright_of(len_row[0:1], batch), upright_of(start_row[0:1], batch)
+    count = lax.broadcasted_iota(jnp.int32, (batch, all_rows), 1).astype(f32)
+    for step in range(steps):
+        hit = jnp.logical_and(count == start_col + step, len_col > step)
+        unpack[step * batch:(step + 1) * batch, :] = jnp.where(hit, 1.0, 0.0).astype(bf16)
+
+    def begin(h):
+        x_src[h] = row_sum(h).astype(bf16)
+        spread_x(h)
+        yield
+        yield from enter(0, h)
+
+    def enter(l, h):
+        k = 2 * l * lots + h
+        forward_x(k)
+        yield
+        weight(0, l)
+        take_x(k)
+        squares = None
+        for p in range(ratio):
+            raw = x_recv[k, p].astype(f32)
+            sq = jnp.sum(raw * raw, axis=1, keepdims=True)
+            squares = sq if squares is None else squares + sq
+            gain = gains[l:l + 1, pl.ds(pl.multiple_of((d * ratio + p) * cols, cols), cols)]
+            norm_buf[h, :, p * cols:(p + 1) * cols] = (raw * gain).astype(bf16)
+        drive = jnp.dot(norm_buf[h], v_drive[l], preferred_element_type=f32)
+        high = squares.astype(bf16)
+        low = (squares - high.astype(f32)).astype(bf16)
+        lane = lax.broadcasted_iota(jnp.int32, (rows, width), 1)
+        tail = jnp.where(
+            lane == 0, high.astype(f32), jnp.where(lane == 1, low.astype(f32), 0.0)
+        ).astype(bf16)
+        k = l * lots + h
         for c in range(nd):
-            top = h * rows + c * chunk
-            part = jnp.dot(pack_own[top:top + chunk, :], tok[...], preferred_element_type=f32)
-            row_send[h, c] = part.astype(bf16)
-            send_row(h, c)
-    for c in range(nd):
-        send(
-            carried.at[:, :, :, pl.ds(c * own_ch, own_ch)], st_recv.at[d],
-            st_ss.at[c], st_rs.at[d], c, t, d == c,
+            a_send[k, c] = jnp.concatenate(
+                [drive[:, c * width:(c + 1) * width].astype(bf16), tail], axis=1
+            )
+            send(a_send.at[k, c], a_recv.at[k, d], a_ss.at[k, c], a_rs.at[k, d], c, t, d == c)
+        yield
+        weight(1, l)
+        send_rows(
+            (1 + 3 * l) * lots + h, jnp.dot(norm_buf[h], v_open[l], preferred_element_type=f32)
         )
-    cols = tok.shape[1]
-    residual = []
-    for h in every:
-        residual.append(row_sum(h).astype(bf16))
-        x_src[h] = residual[h]
-        spread_x(h)
-    for s in range(nd):
-        arrive(st_recv.at[s], st_rs.at[s])
-    for l in range(layers):
-        first, second = 2 * l * lots, (2 * l + 1) * lots
-        k_open = (1 + 3 * l) * lots
-        k_merge, k_exit = k_open + lots, k_open + 2 * lots
-        for h in every:
-            forward_x(first + h)
-        weight(0, l)
-        normed = []
-        for h in every:
-            take_x(first + h)
-            scaled, squares = [], None
-            for p in range(ratio):
-                raw = x_recv[first + h, p].astype(f32)
-                sq = jnp.sum(raw * raw, axis=1, keepdims=True)
-                squares = sq if squares is None else squares + sq
-                scaled.append((raw * gains[l, d, p]).astype(bf16))
-            normed.append(jnp.concatenate(scaled, axis=1))
-            drive = jnp.dot(normed[h], v_drive[l], preferred_element_type=f32)
-            high = squares.astype(bf16)
-            low = (squares - high.astype(f32)).astype(bf16)
-            lane = lax.broadcasted_iota(jnp.int32, (rows, width), 1)
-            tail = jnp.where(
-                lane == 0, high.astype(f32), jnp.where(lane == 1, low.astype(f32), 0.0)
-            ).astype(bf16)
-            k = l * lots + h
-            for c in range(nd):
-                a_send[k, c] = jnp.concatenate(
-                    [drive[:, c * width:(c + 1) * width].astype(bf16), tail], axis=1
-                )
-                send(a_send.at[k, c], a_recv.at[k, d], a_ss.at[k, c], a_rs.at[k, d], c, t, d == c)
-        weight(1, l)
-        for h in every:
-            for c in range(nd):
-                part = jnp.dot(
-                    normed[h][c * chunk:(c + 1) * chunk], v_open[l], preferred_element_type=f32
-                )
-                row_send[k_open + h, c] = part.astype(bf16)
-                send_row(k_open + h, c)
-        feeds = []
+        yield
+
+    def recur(l):
         for h in every:
             k = l * lots + h
             summed = None
@@ -391,115 +464,124 @@
             full_sq = summed[:, width:width + 1] + summed[:, width + 1:width + 2]
             inverse = lax.rsqrt(full_sq / model + EPS)
             inv_buf[h * rows:(h + 1) * rows, :] = jnp.broadcast_to(inverse, (rows, 128))
-            lane2 = lax.broadcasted_iota(jnp.int32, summed.shape, 1)
-            feed = jnp.where(lane2 < width, summed * inverse, jnp.where(lane2 == width, 1.0, 0.0))
-            feeds.append(feed.astype(bf16))
-        feed = jnp.concatenate(feeds, axis=0)
-        real = jnp.concatenate([st_recv[s, l, 0] for s in range(nd)], axis=0)
-        imag = jnp.concatenate([st_recv[s, l, 1] for s in range(nd)], axis=0)
-        dr, di = decay[l, 0, d], decay[l, 1, d]
+            lane = lax.broadcasted_iota(jnp.int32, summed.shape, 1)
+            feed = jnp.where(lane < width, summed * inverse, jnp.where(lane == width, 1.0, 0.0))
+            feed_buf[h * rows:(h + 1) * rows, :] = feed.astype(bf16)
+        for s in range(nd):
+            arrive(st_recv.at[l, s], st_rs.at[l, s])
+        real = jnp.concatenate([st_recv[l, s, 0] for s in range(nd)], axis=0)
+        imag = jnp.concatenate([st_recv[l, s, 1] for s in range(nd)], axis=0)
+        dr, di, gap = decays(l, 0), decays(l, 1), skips(l)
         for step in range(steps):
             span = slice(step * batch, (step + 1) * batch)
-            u = jnp.dot(unpack[span, :], feed, preferred_element_type=f32)
+            u = jnp.dot(unpack[span, :], feed_buf[...], preferred_element_type=f32)
             live = u[:, width:width + 1] > 0.5
-            push = jnp.dot(u.astype(bf16), inject[l, d], preferred_element_type=f32)
+            push = jnp.dot(u.astype(bf16), inj[l], preferred_element_type=f32)
             moved_real = dr * real - di * imag + push[:, :own_ch]
             moved_imag = dr * imag + di * real + push[:, own_ch:]
             real = jnp.where(live, moved_real, real)
             imag = jnp.where(live, moved_imag, imag)
             both = jnp.concatenate([real, imag], axis=1).astype(bf16)
-            read = jnp.dot(both, outmix[l, d], preferred_element_type=f32) + skip[l, d] * u
+            read = lax.dot_general(
+                both, omx[l], (((1,), (1,)), ((), ())), preferred_element_type=f32
+            ) + gap * u
             act_buf[span, :] = jax.nn.gelu(read).astype(bf16)
         st_new[l, 0] = real
         st_new[l, 1] = imag
-        packed_all = turned(unpack[...], act_buf[...]).astype(bf16)
-        activated = []
-        for h in every:
-            packed = packed_all[h * rows:(h + 1) * rows]
-            activated.append(fold(packed[:, :width]))
-            y_src[first + h] = activated[h]
-            spread_y(first + h)
-        for h in every:
-            mine = pl.ds(pl.multiple_of(h * rows + d * chunk, chunk), chunk)
-            gate_buf[h] = jax.nn.sigmoid(row_sum(k_open + h) * inv_buf[mine, 0:1])
+
+    def chain(l, h):
+        first, second = 2 * l * lots + h, (2 * l + 1) * lots + h
+        k_open = (1 + 3 * l) * lots + h
+        k_merge, k_exit = k_open + lots, k_open + 2 * lots
+        packed = turned(unpack[:, h * rows:(h + 1) * rows], act_buf[...]).astype(bf16)
+        y_src[first] = fold(packed[:, :width])
+        spread_y(first)
+        yield
+        forward_y(first)
+        yield
         weight(2, l)
-        for h in every:
-            forward_y(first + h)
-        for h in every:
-            wide = take_y(first + h)
-            gating = jnp.dot(wide, v_glu[l], preferred_element_type=f32).astype(bf16)
-            k = l * lots + h
+        gating = jnp.dot(take_y(first), v_glu[l], preferred_element_type=f32).astype(bf16)
+        k = l * lots + h
+        for c in range(nd):
+            c_send[k, c] = fold(gating[:, c * width:(c + 1) * width])
+            send(c_send.at[k, c], c_recv.at[k, d], c_ss.at[k, c], c_rs.at[k, d], c, t, d == c)
+        yield
+        summed = None
+        for s in range(nd):
+            arrive(c_recv.at[k, s], c_rs.at[k, s])
+            v = c_recv[k, s].astype(f32)
+            summed = v if summed is None else summed + v
+        y_src[second] = (y_src[first].astype(f32) * jax.nn.sigmoid(summed)).astype(bf16)
+        spread_y(second)
+        yield
+        forward_y(second)
+        yield
+        weight(3, l)
+        send_rows(k_merge, jnp.dot(take_y(second), v_merge[l], preferred_element_type=f32))
+        yield
+        mine = pl.ds(pl.multiple_of(h * rows + d * chunk, chunk), chunk)
+        gate = jax.nn.sigmoid(row_sum(k_open) * inv_buf[mine, 0:1])
+        x_src[second] = (gate * row_sum(k_merge)).astype(bf16)
+        spread_x(second)
+        yield
+        forward_x(second)
+        yield
+        weight(4, l)
+        take_x(second)
+        part = None
+        for p in range(ratio):
+            v = jnp.dot(
+                x_recv[second, p], v_exit[l, p * cols:(p + 1) * cols], preferred_element_type=f32
+            )
+            part = v if part is None else part + v
+        send_rows(k_exit, part)
+        yield
+        k = (2 * l + 2) * lots + h
+        x_src[k] = (x_src[first].astype(f32) + row_sum(k_exit)).astype(bf16)
+        if l + 1 < layers:
+            spread_x(k)
+            yield
+            yield from enter(l + 1, h)
+        else:
             for c in range(nd):
-                c_send[k, c] = fold(gating[:, c * width:(c + 1) * width])
-                send(c_send.at[k, c], c_recv.at[k, d], c_ss.at[k, c], c_rs.at[k, d], c, t, d == c)
-        for h in every:
-            k = l * lots + h
-            summed = None
-            for s in range(nd):
-                arrive(c_recv.at[k, s], c_rs.at[k, s])
-                v = c_recv[k, s].astype(f32)
-                summed = v if summed is None else summed + v
-            gated = activated[h].astype(f32) * jax.nn.sigmoid(summed)
-            y_src[second + h] = gated.astype(bf16)
-            spread_y(second + h)
-        weight(3, l)
-        for h in every:
-            forward_y(second + h)
-        for h in every:
-            wide = take_y(second + h)
-            for c in range(nd):
-                part = jnp.dot(
-                    wide[c * chunk:(c + 1) * chunk], v_merge[l], preferred_element_type=f32
+                send(
+                    x_src.at[k], fin_recv.at[pl.ds(h * rows + d * chunk, chunk)],
+                    f_ss.at[h, c], f_rs.at[h, d], c, t, d == c,
                 )
-                row_send[k_merge + h, c] = part.astype(bf16)
-                send_row(k_merge + h, c)
-        for h in every:
-            x_src[second + h] = (gate_buf[h] * row_sum(k_merge + h)).astype(bf16)
-            spread_x(second + h)
-        for c in range(nd):
-            send(
-                st_new.at[l, :, pl.ds(c * batch_own, batch_own)], nst_recv.at[d, l],
-                n_ss.at[l, c], n_rs.at[l, d], c, t, d == c,
-            )
-        weight(4, l)
-        for h in every:
-            forward_x(second + h)
-        for h in every:
-            take_x(second + h)
-            for c in range(nd):
-                part = None
-                for p in range(ratio):
-                    v = jnp.dot(
-                        x_recv[second + h, p, c * chunk:(c + 1) * chunk],
-                        v_exit[l, p * cols:(p + 1) * cols],
-                        preferred_element_type=f32,
-                    )
-                    part = v if part is None else part + v
-                row_send[k_exit + h, c] = part.astype(bf16)
-                send_row(k_exit + h, c)
-        for h in every:
-            residual[h] = (residual[h].astype(f32) + row_sum(k_exit + h)).astype(bf16)
-            k = (2 * l + 2) * lots + h
-            x_src[k] = residual[h]
-            if l + 1 < layers:
-                spread_x(k)
-            else:
-                for c in range(nd):
-                    send(
-                        x_src.at[k], fin_recv.at[pl.ds(h * rows + d * chunk, chunk)],
-                        f_ss.at[h, c], f_rs.at[h, d], c, t, d == c,
-                    )
+            yield
+
+    def run(gens, hooks):
+        live, turn_count = list(range(lots)), 0
+        while live:
+            for h in list(live):
+                if turn_count >= h * SKEW:
+                    try:
+                        next(gens[h])
+                    except StopIteration:
+                        live.remove(h)
+            if turn_count in hooks:
+                hooks.pop(turn_count)()
+            turn_count += 1
+        for rest in hooks.values():
+            rest()
+
+    run([begin(h) for h in every], {2 * SKEW: lambda: send_states(0)})
+    for l in range(layers):
+        recur(l)
+        hooks = {4: functools.partial(return_states, l)}
+        if l + 1 < layers:
+            hooks[7] = functools.partial(send_states, l + 1)
+        run([chain(l, h) for h in every], hooks)
     for l in range(layers):
         for s in range(nd):
-            arrive(nst_recv.at[s, l], n_rs.at[l, s])
-            for part in range(2):
-                out_state[l, part, :, s * own_ch:(s + 1) * own_ch] = nst_recv[s, l, part]
+            into = out_state.at[l, :, :, pl.ds(s * own_ch, own_ch)]
+            arrive(into, n_rs.at[l, s])
     for h in every:
         for s in range(nd):
             arrive(fin_recv.at[pl.ds(h * rows + s * chunk, chunk)], f_rs.at[h, s])
     spread = turned(pack_own[...], fin_recv[...])
     keep = turned(pack_own[...], jnp.ones((all_rows, 128), bf16))[:, 0:1]
-    out_tok[...] = jnp.where(keep > 0.5, spread, tok[...].astype(f32)).astype(bf16)
+    out_tok[...] = jnp.where(keep > 0.5, spread, v_tok[...].astype(f32)).astype(bf16)
     for far, is_self in pending:
         if is_self is None:
             far.wait_send()
@@ -513,7 +595,6 @@
 ):
     f32, bf16 = jnp.float32, jnp.bfloat16
     nd, nt = lax.axis_size("dp"), lax.axis_size("tp")
-    d, t = lax.axis_index("dp"), lax.axis_index("tp")
     layers = norm_gains.shape[0]
     own, steps, cols = tokens.shape
     batch = own * nd
@@ -528,45 +609,7 @@
     own_ch = few * entries
     chunk = rows // nd
 
-    place = jnp.arange(batch, dtype=jnp.int32) // own
-    lens = jnp.where(place == d, jnp.tile(lengths, nd), 0).astype(f32)
-    lens = jnp.broadcast_to(lens[None, :], (8, batch))
-    gains = norm_gains.reshape(layers, nd, ratio, 1, cols)
-
-    real_eig = -decay_rate
-    turn_now = turn_rate
-    step_len = group_step_width[..., None]
-    in_pair, out_pair = state_in, state_out
-    skip_now = skip_gain.reshape(layers, nd, 1, width)
-    magnitude = jnp.exp(step_len * real_eig)
-    decay_real = magnitude * jnp.cos(step_len * turn_now)
-    decay_imag = magnitude * jnp.sin(step_len * turn_now)
-    divisor = real_eig * real_eig + turn_now * turn_now
-    hold_real = ((decay_real - 1.0) * real_eig + decay_imag * turn_now) / divisor
-    hold_imag = (decay_imag * real_eig - (decay_real - 1.0) * turn_now) / divisor
-    inject_real = hold_real[..., None] * in_pair[:, 0] - hold_imag[..., None] * in_pair[:, 1]
-    inject_imag = hold_real[..., None] * in_pair[:, 1] + hold_imag[..., None] * in_pair[:, 0]
-    eye = jnp.eye(few, dtype=f32)
-    both = jnp.stack([inject_real, inject_imag], axis=1).reshape(
-        layers, 2, nd, few, entries, members
-    )
-    inject = (
-        jnp.transpose(both, (0, 2, 3, 5, 1, 4))[:, :, :, :, :, None, :]
-        * eye[None, None, :, None, None, :, None]
-    ).reshape(layers, nd, width, 2 * own_ch)
-    inject = jnp.pad(inject, ((0, 0), (0, 0), (0, width), (0, 0))).astype(bf16)
-    signed = jnp.stack([out_pair[:, 0], -out_pair[:, 1]], axis=1).reshape(
-        layers, 2, nd, few, members, entries
-    )
-    outmix = (
-        jnp.transpose(signed, (0, 2, 1, 3, 5, 4))[:, :, :, :, :, None, :]
-        * eye[None, None, None, :, None, :, None]
-    ).reshape(layers, nd, 2 * own_ch, width)
-    outmix = jnp.pad(outmix, ((0, 0), (0, 0), (0, 0), (0, width))).astype(bf16)
-    skip = jnp.pad(skip_now, ((0, 0), (0, 0), (0, 0), (0, width)))
-    decay = jnp.stack([decay_real, decay_imag], axis=1).reshape(layers, 2, nd, 1, own_ch)
-
-    lots = 3
+    lots = LOTS
     n_row = (1 + 3 * layers) * lots
     n_col = layers * lots
     n_all = 2 * layers * lots
@@ -577,6 +620,13 @@
     dma = pltpu.SemaphoreType.DMA
     weights = (drive_proj, open_proj, glu_proj, merge_proj, exit_proj)
     scratch = [vm(w.shape, bf16) for w in weights] + [
+        vm((own * steps, cols), bf16),
+        vm((layers, 2, few, members, entries), f32),
+        vm((layers, 2, few, members, entries), f32),
+        vm((layers, 4, groups_own, entries), f32),
+        vm((layers, 2 * width, 2 * own_ch), bf16),
+        vm((layers, 2 * width, 2 * own_ch), bf16),
+        vm((8, batch), f32),
         vm((n_row, nd, piece, cols), bf16),
         vm((n_row, nd, piece, cols), bf16),
         vm((n_col, nd, lot, 2 * width), bf16),
@@ -587,23 +637,23 @@
         vm((n_all, ratio, lot, cols), bf16),
         vm((n_all, half, 2 * width), bf16),
         vm((n_all, nt, half, 2 * width), bf16),
-        vm((nd, layers, 2, own, own_ch), f32),
+        vm((layers, nd, 2, own, own_ch), f32),
         vm((layers, 2, batch, own_ch), f32),
-        vm((nd, layers, 2, own, own_ch), f32),
         vm((rows, cols), bf16),
+        vm((lots, lot, ratio * cols), bf16),
         vm((rows, 128), f32),
-        vm((lots, piece, cols), f32),
         vm((steps * batch, 2 * width), bf16),
+        vm((rows, 2 * width), bf16),
         vm((nd, 8, batch), f32),
         vm((rows, own * steps), bf16),
         vm((steps * batch, rows), bf16),
-        dma((5, layers)),
+        dma((5, layers)), dma((3,)),
         dma((n_row, nd)), dma((n_row, nd)),
         dma((n_col, nd)), dma((n_col, nd)),
         dma((n_col, nd)), dma((n_col, nd)),
         dma((n_all, nd * ratio)), dma((n_all, nt)),
         dma((n_all, nd * ratio)), dma((n_all, nt)),
-        dma((nd,)), dma((nd,)),
+        dma((layers, nd)), dma((layers, nd)),
         dma((layers, nd)), dma((layers, nd)),
         dma((lots, nd)), dma((lots, nd)),
         dma((nd,)), dma((nd,)),
@@ -616,15 +666,16 @@
             jax.ShapeDtypeStruct((own * steps, cols), bf16),
             jax.ShapeDtypeStruct(carried_state.shape, f32),
         ),
-        in_specs=[inside] * 8 + [outside] * 5,
-        out_specs=(inside, inside),
+        in_specs=[outside] + [inside] * 5 + [outside] * 2 + [inside] + [outside] * 6,
+        out_specs=(inside, outside),
         scratch_shapes=scratch,
         compiler_params=pltpu.CompilerParams(
             collective_id=0, has_side_effects=True, vmem_limit_bytes=60 * 1024 * 1024
         ),
     )(
-        tokens.reshape(own * steps, cols), lens,
-        gains, decay, inject, outmix, skip, carried_state, *weights,
+        tokens.reshape(own * steps, cols), lengths.reshape(1, own),
+        norm_gains, decay_rate, turn_rate, group_step_width,
+        jnp.swapaxes(state_in, 3, 4), state_out, skip_gain, carried_state, *weights,
     )
     return out_rows.reshape(own, steps, cols), out_state
 

time: 174 us -> 155 us (0.89)
  local copies, waits for them, and re-layouts: 16.5 us -> 3.55 us
  Pallas kernels: 155 us -> 150 us
  other arithmetic: 2.02 us -> 0 us
    mul x10 -> x0, local copies, waits for them, and re-layouts: 4.8 us -> none  [the longest x6 2.81 us: fused_shards(): jnp.transpose(signed, (0, 2, 1, 3, 5, 4))[:, :, :, :, :, None, :]]
    pallas_call x1, Pallas kernels: 155 us -> 150 us  [fused_shards(): pl.pallas_call(functools.partial(fused_kernel, (layers, nd, nt, rows, mod...]
    pad x3 -> x0, local copies, waits for them, and re-layouts: 2.91 us -> none  [the longest x1 1.25 us: fused_shards(): outmix = jnp.pad(outmix, ((0, 0), (0, 0), (0, 0), (0, width))).astype(bf16)]
    reshape x2 -> x0, local copies, waits for them, and re-layouts: 2.19 us -> none  [the longest x1 1.42 us: fused_shards(): gains = norm_gains.reshape(layers, nd, ratio, 1, cols)]
    unnamed x8 -> x2, local copies, waits for them, and re-layouts: 3.57 us -> 3.55 us
where the time goes in v1:
time: 155 us; the launch traced here: 154 us
  Pallas kernels  150 us (97%)
  local copies, waits for them, and re-layouts  3.55 us (2%)
    pallas_call x1, Pallas kernels, fused_shards(): pl.pallas_call(functools.partial(fused_kernel, (layers, nd, nt, rows, mod...  150 us
    unnamed x2, local copies, waits for them, and re-layouts  3.55 us

profile of v1, /device:TPU:0, one launch (start us, length us, event | category | flops | bytes accessed | tf_op | source)
XLA Modules:
  0.0 154.3 jit_solution(2633669160855614269)
XLA Ops:
  0.6 150.1 %shard_map.158 = (bf16[256,512]{1,0:T(8,128)(2,1)}, f32[2,2,32,1024]{3,2,1,0:T(8,128)}) custom-call(bf16[256,512]{1,0:T(8,128)(2,1)} %bitcast.6, s32[1,32]{1,0:T(1,128)} %bitcast.7, f32[2,4096]{1,0:T(2,128)} %gains.1, f32[2,16,64]{2,1,0:T(8,128)} %rate.1, f32[2,16,64]{2,1,0:T(8,128)} %turn.1, f32[2,16]{1,0:T(2,128)} %size.1, f32[2,2,16,16,64]{4,3,2,1,0:T(8,128)} %bitcast.4, ...), custom_call_target="tpu_custom_call" | custom-call | tf_op jit(solution)/shard_map/pallas_call | solution.py:663
  150.7 1.7 %copy.19 = bf16[32,8,512]{2,1,0:T(8,128)(2,1)} copy(bf16[32,8,512]{2,1,0:T(8,128)(2,1)} %bitcast.5) | data formatting | bytes 524288
  152.4 1.9 %copy.20 = f32[2,2,32,1024]{3,2,1,0:T(8,128)} copy(f32[2,2,32,1024]{3,2,1,0:T(8,128)} %get-tuple-element.9) | data formatting | bytes 1048576

commit v2 on v1

--- a/solution.py
+++ b/solution.py
@@ -131,8 +131,9 @@
     return (residual.reshape(sequences, positions, local_width), jnp.stack(states))
 
 
-LOTS = 3
-SKEW = 0
+LOTS = 6
+MIXED = 1
+ROW, COL, ST, LEN, FIN, XF, YF, LANES = 0, 1, 3, 5, 6, 7, 13, 19
 
 
 def fused_kernel(
@@ -143,10 +144,9 @@
     v_drive, v_open, v_glu, v_merge, v_exit, v_tok, v_in, v_out,
     par, inj, omx, len_own,
     row_send, row_recv, a_send, a_recv, c_send, c_recv,
-    x_src, x_recv, y_src, y_recv, st_recv, st_new, fin_recv,
+    x_src, x_near, x_recv, y_src, y_near, y_recv, st_recv, st_new, fin_recv,
     norm_buf, inv_buf, act_buf, feed_buf, len_recv, pack_own, unpack,
-    w_sem, in_sem, row_ss, row_rs, a_ss, a_rs, c_ss, c_rs, x_ss, x_rs, y_ss, y_rs,
-    st_ss, st_rs, n_ss, n_rs, f_ss, f_rs, l_ss, l_rs,
+    w_sem, in_sem, row_rs, a_rs, c_rs, x_rs, y_rs, xn_rs, yn_rs, st_rs, n_rs, f_rs, l_rs, out_sem,
 ):
     layers, nd, nt, all_rows, model, lots = dims
     ratio = nt // nd
@@ -202,98 +202,99 @@
         if (i, l) in loads:
             loads.pop((i, l)).wait()
 
-    pending = []
-
-    def send(src, dst, ss, rs, to_dp, to_tp, is_self):
-        far = pltpu.make_async_remote_copy(
-            src_ref=src, dst_ref=dst, send_sem=ss, recv_sem=rs,
+    def send(src, dst, rs, to_dp, to_tp, lane):
+        copy = pltpu.make_async_remote_copy(
+            src_ref=src, dst_ref=dst, send_sem=out_sem.at[lane], recv_sem=rs,
             device_id={"tp": to_tp, "dp": to_dp}, device_id_type=pl.DeviceIdType.MESH,
         )
-        if is_self is None:
-            far.start()
-        else:
-            @pl.when(is_self)
-            def _():
-                pltpu.make_async_copy(src, dst, rs).start()
-
-            @pl.when(jnp.logical_not(is_self))
-            def _():
-                far.start()
-
-        pending.append((far, is_self))
+        copy.start()
 
     def arrive(dst, rs):
         pltpu.make_async_copy(dst, dst, rs).wait()
 
-    def send_row(k, c):
-        send(row_send.at[k, c], row_recv.at[k, d], row_ss.at[k, c], row_rs.at[k, d], c, t, d == c)
+    others = [(j, lax.rem(d + j, nd)) for j in range(1, nd)]
+
+    def trade(src, dst, rs, lane):
+        for j, to in others:
+            send(src.at[to], dst.at[j - 1], rs, to, t, lane)
+
+    def traded(src, dst, rs):
+        arrive(dst, rs)
+        acc = src[d].astype(f32)
+        for j in range(nd - 1):
+            acc = acc + dst[j].astype(f32)
+        return acc
 
     def row_sum(k):
-        acc = None
-        for s in range(nd):
-            arrive(row_recv.at[k, s], row_rs.at[k, s])
-            v = row_recv[k, s].astype(f32)
-            acc = v if acc is None else acc + v
-        return acc
+        return traded(row_send.at[k], row_recv.at[k], row_rs.at[k])
 
     def send_rows(k, part):
         part = part.astype(bf16)
         for c in range(nd):
             row_send[k, c] = part[c * chunk:(c + 1) * chunk]
-            send_row(k, c)
-
-    def spread_x(k):
-        slot = place * nd + d
-        for j in range(nd):
-            to = lax.rem(home + j, nd) * ratio + place
-            send(
-                x_src.at[k], x_recv.at[k, place, pl.ds(d * chunk, chunk)],
-                x_ss.at[k, j], x_rs.at[k, slot], home, to, (d == home) if j == 0 else None,
-            )
-
-    def forward_x(k):
-        for s in range(nd):
-            piece = x_recv.at[k, place, pl.ds(s * chunk, chunk)]
-            arrive(piece, x_rs.at[k, place * nd + s])
+        trade(row_send.at[k], row_recv.at[k], row_rs.at[k], ROW)
+
+    def fan(src, dst, rs, lane):
+        for j in range(1, nd):
+            send(src, dst, rs, home, lax.rem(home + j, nd) * ratio + place, lane)
+
+        @pl.when(d == home)
+        def _():
+            pltpu.make_async_copy(src, dst, rs).start()
+
+        @pl.when(d != home)
+        def _():
+            send(src, dst, rs, home, t, lane + 1)
+
+    def aside(src, near, rs, lane):
+        for i in range(1, ratio):
+            p = lax.rem(place + i, ratio)
+            send(src, near.at[i - 1], rs.at[i - 1], d, home * ratio + p, lane)
+
+    def x_slot(k, p):
+        return x_recv.at[k, p, pl.ds(d * chunk, chunk)]
+
+    def y_slot(k, p):
+        return y_recv.at[k, p * nd + d]
+
+    def x_whole(k, p):
+        return x_recv.at[k, p]
+
+    def y_whole(k, p):
+        return y_recv.at[k, pl.ds(p * nd, nd)]
+
+    X = (x_src, x_near, x_slot, x_whole, x_rs, xn_rs, XF)
+    Y = (y_src, y_near, y_slot, y_whole, y_rs, yn_rs, YF)
+
+    def spread(kind, k, near_first):
+        src, near, slot, whole, rs, near_rs, lane = kind
+        if near_first:
+            aside(src.at[k], near.at[k], near_rs.at[k], lane + 3)
+        else:
+            fan(src.at[k], slot(k, place), rs.at[k, place], lane)
+
+    def forward(kind, k, near_first):
+        src, near, slot, whole, rs, near_rs, lane = kind
+        if near_first:
+            fan(src.at[k], slot(k, place), rs.at[k, place], lane)
+            for i in range(1, ratio):
+                p = lax.rem(place + ratio - i, ratio)
+                arrive(near.at[k, i - 1], near_rs.at[k, i - 1])
+                fan(near.at[k, i - 1], slot(k, p), rs.at[k, p], lane + 4)
+        else:
+            arrive(whole(k, place), rs.at[k, place])
             for i in range(1, ratio):
                 to = home * ratio + lax.rem(place + i, ratio)
-                send(
-                    piece, piece, x_ss.at[k, nd + s * (ratio - 1) + i - 1],
-                    x_rs.at[k, place * nd + s], d, to, None,
-                )
-
-    def take_x(k):
-        for i in range(1, ratio):
+                send(whole(k, place), whole(k, place), rs.at[k, place], d, to, lane + 2)
+
+    def take(kind, k, near_first):
+        src, near, slot, whole, rs, near_rs, lane = kind
+        for i in range(0 if near_first else 1, ratio):
             p = lax.rem(place + i, ratio)
-            for s in range(nd):
-                arrive(x_recv.at[k, p, pl.ds(s * chunk, chunk)], x_rs.at[k, p * nd + s])
-
-    def spread_y(k):
-        slot = place * nd + d
-        for j in range(nd):
-            to = lax.rem(home + j, nd) * ratio + place
-            send(
-                y_src.at[k], y_recv.at[k, slot],
-                y_ss.at[k, j], y_rs.at[k, slot], home, to, (d == home) if j == 0 else None,
-            )
-
-    def forward_y(k):
-        for s in range(nd):
-            slot = place * nd + s
-            piece = y_recv.at[k, slot]
-            arrive(piece, y_rs.at[k, slot])
-            for i in range(1, ratio):
-                to = home * ratio + lax.rem(place + i, ratio)
-                send(
-                    piece, piece, y_ss.at[k, nd + s * (ratio - 1) + i - 1],
-                    y_rs.at[k, slot], d, to, None,
-                )
-
-    def take_y(k):
-        for i in range(1, ratio):
-            p = lax.rem(place + i, ratio)
-            for s in range(nd):
-                arrive(y_recv.at[k, p * nd + s], y_rs.at[k, p * nd + s])
+            arrive(whole(k, p), rs.at[k, p])
+
+    def take_y(k, near_first):
+        take(Y, k, near_first)
         parts = []
         for p in range(ratio):
             for s in range(nd):
@@ -304,20 +305,23 @@
     def fold(v):
         return jnp.concatenate([v[:half], v[half:]], axis=1)
 
+    def own_span(c):
+        return pl.ds(pl.multiple_of(c * own_ch, own_ch), own_ch)
+
     def send_states(l):
-        for c in range(nd):
-            send(
-                carried.at[l, :, :, pl.ds(c * own_ch, own_ch)], st_recv.at[l, d],
-                st_ss.at[l, c], st_rs.at[l, d], c, t, d == c,
-            )
+        into = st_recv.at[l, d]
+        pltpu.make_async_copy(carried.at[l, :, :, own_span(d)], into, st_rs.at[l]).start()
+        for j, to in others:
+            send(carried.at[l, :, :, own_span(to)], into, st_rs.at[l], to, t, ST)
 
     def return_states(l):
-        for c in range(nd):
-            send(
-                st_new.at[l, :, pl.ds(c * batch_own, batch_own)],
-                out_state.at[l, :, :, pl.ds(pl.multiple_of(d * own_ch, own_ch), own_ch)],
-                n_ss.at[l, c], n_rs.at[l, d], c, t, d == c,
-            )
+        def rows_of(c):
+            return st_new.at[l, :, pl.ds(pl.multiple_of(c * batch_own, batch_own), batch_own)]
+
+        into = out_state.at[l, :, :, own_span(d)]
+        pltpu.make_async_copy(rows_of(d), into, n_rs.at[l]).start()
+        for j, to in others:
+            send(rows_of(to), into, n_rs.at[l], to, t, ST + 1)
 
     wide = jnp.concatenate([lens[...].astype(f32)] * nd, axis=1)
     owner = lax.broadcasted_iota(jnp.int32, wide.shape, 1) // batch_own
@@ -341,8 +345,8 @@
         par[l, 3] = (decay_imag * real_eig - (decay_real - 1.0) * turn_now) / divisor
 
     pl.semaphore_wait(barrier, total - 1)
-    for c in range(nd):
-        send(len_own, len_recv.at[d], l_ss.at[c], l_rs.at[d], c, t, d == c)
+    for j, to in others:
+        send(len_own, len_recv.at[j - 1], l_rs.at[0], to, t, LEN)
 
     in_load.wait()
     out_load.wait()
@@ -374,10 +378,10 @@
             own = v if own is None else jnp.where(d == s, v, own)
         return jnp.concatenate([own, jnp.zeros_like(own)], axis=1)
 
-    len_row = None
-    for s in range(nd):
-        arrive(len_recv.at[s], l_rs.at[s])
-        len_row = len_recv[s] if len_row is None else len_row + len_recv[s]
+    arrive(len_recv, l_rs.at[0])
+    len_row = len_own[...]
+    for s in range(nd - 1):
+        len_row = len_row + len_recv[s]
     down = lax.broadcasted_iota(jnp.int32, (batch, batch), 0)
     along = lax.broadcasted_iota(jnp.int32, (batch, batch), 1)
     before = jnp.where(down < along, 1.0, 0.0).astype(bf16)
@@ -414,18 +418,21 @@
         hit = jnp.logical_and(count == start_col + step, len_col > step)
         unpack[step * batch:(step + 1) * batch, :] = jnp.where(hit, 1.0, 0.0).astype(bf16)
 
+    def near(gather, h):
+        return (h - gather) % lots < MIXED
+
     def begin(h):
         x_src[h] = row_sum(h).astype(bf16)
-        spread_x(h)
+        spread(X, h, near(0, h))
         yield
         yield from enter(0, h)
 
     def enter(l, h):
         k = 2 * l * lots + h
-        forward_x(k)
+        forward(X, k, near(4 * l, h))
         yield
         weight(0, l)
-        take_x(k)
+        take(X, k, near(4 * l, h))
         squares = None
         for p in range(ratio):
             raw = x_recv[k, p].astype(f32)
@@ -445,7 +452,7 @@
             a_send[k, c] = jnp.concatenate(
                 [drive[:, c * width:(c + 1) * width].astype(bf16), tail], axis=1
             )
-            send(a_send.at[k, c], a_recv.at[k, d], a_ss.at[k, c], a_rs.at[k, d], c, t, d == c)
+        trade(a_send.at[k], a_recv.at[k], a_rs.at[k], COL)
         yield
         weight(1, l)
         send_rows(
@@ -456,19 +463,14 @@
     def recur(l):
         for h in every:
             k = l * lots + h
-            summed = None
-            for s in range(nd):
-                arrive(a_recv.at[k, s], a_rs.at[k, s])
-                v = a_recv[k, s].astype(f32)
-                summed = v if summed is None else summed + v
+            summed = traded(a_send.at[k], a_recv.at[k], a_rs.at[k])
             full_sq = summed[:, width:width + 1] + summed[:, width + 1:width + 2]
             inverse = lax.rsqrt(full_sq / model + EPS)
             inv_buf[h * rows:(h + 1) * rows, :] = jnp.broadcast_to(inverse, (rows, 128))
             lane = lax.broadcasted_iota(jnp.int32, summed.shape, 1)
             feed = jnp.where(lane < width, summed * inverse, jnp.where(lane == width, 1.0, 0.0))
             feed_buf[h * rows:(h + 1) * rows, :] = feed.astype(bf16)
-        for s in range(nd):
-            arrive(st_recv.at[l, s], st_rs.at[l, s])
+        arrive(st_recv.at[l], st_rs.at[l])
         real = jnp.concatenate([st_recv[l, s, 0] for s in range(nd)], axis=0)
         imag = jnp.concatenate([st_recv[l, s, 1] for s in range(nd)], axis=0)
         dr, di, gap = decays(l, 0), decays(l, 1), skips(l)
@@ -495,39 +497,37 @@
         k_merge, k_exit = k_open + lots, k_open + 2 * lots
         packed = turned(unpack[:, h * rows:(h + 1) * rows], act_buf[...]).astype(bf16)
         y_src[first] = fold(packed[:, :width])
-        spread_y(first)
-        yield
-        forward_y(first)
+        spread(Y, first, near(4 * l + 1, h))
+        yield
+        forward(Y, first, near(4 * l + 1, h))
         yield
         weight(2, l)
-        gating = jnp.dot(take_y(first), v_glu[l], preferred_element_type=f32).astype(bf16)
+        wide = take_y(first, near(4 * l + 1, h))
+        gating = jnp.dot(wide, v_glu[l], preferred_element_type=f32).astype(bf16)
         k = l * lots + h
         for c in range(nd):
             c_send[k, c] = fold(gating[:, c * width:(c + 1) * width])
-            send(c_send.at[k, c], c_recv.at[k, d], c_ss.at[k, c], c_rs.at[k, d], c, t, d == c)
-        yield
-        summed = None
-        for s in range(nd):
-            arrive(c_recv.at[k, s], c_rs.at[k, s])
-            v = c_recv[k, s].astype(f32)
-            summed = v if summed is None else summed + v
+        trade(c_send.at[k], c_recv.at[k], c_rs.at[k], COL + 1)
+        yield
+        summed = traded(c_send.at[k], c_recv.at[k], c_rs.at[k])
         y_src[second] = (y_src[first].astype(f32) * jax.nn.sigmoid(summed)).astype(bf16)
-        spread_y(second)
-        yield
-        forward_y(second)
+        spread(Y, second, near(4 * l + 2, h))
+        yield
+        forward(Y, second, near(4 * l + 2, h))
         yield
         weight(3, l)
-        send_rows(k_merge, jnp.dot(take_y(second), v_merge[l], preferred_element_type=f32))
+        wide = take_y(second, near(4 * l + 2, h))
+        send_rows(k_merge, jnp.dot(wide, v_merge[l], preferred_element_type=f32))
         yield
         mine = pl.ds(pl.multiple_of(h * rows + d * chunk, chunk), chunk)
         gate = jax.nn.sigmoid(row_sum(k_open) * inv_buf[mine, 0:1])
         x_src[second] = (gate * row_sum(k_merge)).astype(bf16)
-        spread_x(second)
-        yield
-        forward_x(second)
+        spread(X, second, near(4 * l + 3, h))
+        yield
+        forward(X, second, near(4 * l + 3, h))
         yield
         weight(4, l)
-        take_x(second)
+        take(X, second, near(4 * l + 3, h))
         part = None
         for p in range(ratio):
             v = jnp.dot(
@@ -539,54 +539,78 @@
         k = (2 * l + 2) * lots + h
         x_src[k] = (x_src[first].astype(f32) + row_sum(k_exit)).astype(bf16)
         if l + 1 < layers:
-            spread_x(k)
+            spread(X, k, near(4 * l + 4, h))
             yield
             yield from enter(l + 1, h)
         else:
-            for c in range(nd):
-                send(
-                    x_src.at[k], fin_recv.at[pl.ds(h * rows + d * chunk, chunk)],
-                    f_ss.at[h, c], f_rs.at[h, d], c, t, d == c,
-                )
+            into = fin_recv.at[pl.ds(pl.multiple_of(h * rows + d * chunk, chunk), chunk)]
+            pltpu.make_async_copy(x_src.at[k], into, f_rs.at[h]).start()
+            for j, to in others:
+                send(x_src.at[k], into, f_rs.at[h], to, t, FIN)
             yield
 
-    def run(gens, hooks):
-        live, turn_count = list(range(lots)), 0
+    def run(gather, gens, hooks):
+        live, stage = set(every), 0
         while live:
-            for h in list(live):
-                if turn_count >= h * SKEW:
+            turn_of = gather + (stage + 1) // 3
+            for i in every:
+                h = (turn_of + i) % lots
+                if h in live:
                     try:
                         next(gens[h])
                     except StopIteration:
                         live.remove(h)
-            if turn_count in hooks:
-                hooks.pop(turn_count)()
-            turn_count += 1
+            if stage in hooks:
+                hooks.pop(stage)()
+            stage += 1
         for rest in hooks.values():
             rest()
 
-    run([begin(h) for h in every], {2 * SKEW: lambda: send_states(0)})
+    run(0, [begin(h) for h in every], {0: lambda: send_states(0)})
     for l in range(layers):
         recur(l)
-        hooks = {4: functools.partial(return_states, l)}
+        hooks = {10 if l + 1 < layers else 7: functools.partial(return_states, l)}
         if l + 1 < layers:
             hooks[7] = functools.partial(send_states, l + 1)
-        run([chain(l, h) for h in every], hooks)
-    for l in range(layers):
-        for s in range(nd):
-            into = out_state.at[l, :, :, pl.ds(s * own_ch, own_ch)]
-            arrive(into, n_rs.at[l, s])
+        run(4 * l + 1, [chain(l, h) for h in every], hooks)
     for h in every:
-        for s in range(nd):
-            arrive(fin_recv.at[pl.ds(h * rows + s * chunk, chunk)], f_rs.at[h, s])
+        arrive(fin_recv.at[pl.ds(h * rows, rows)], f_rs.at[h])
     spread = turned(pack_own[...], fin_recv[...])
     keep = turned(pack_own[...], jnp.ones((all_rows, 128), bf16))[:, 0:1]
     out_tok[...] = jnp.where(keep > 0.5, spread, v_tok[...].astype(f32)).astype(bf16)
-    for far, is_self in pending:
-        if is_self is None:
-            far.wait_send()
-        else:
-            pl.when(jnp.logical_not(is_self))(far.wait_send)
+    for l in range(layers):
+        arrive(out_state.at[l], n_rs.at[l])
+
+    def sent(like, lane):
+        pltpu.make_async_copy(like, like, out_sem.at[lane]).wait()
+
+    sent(row_recv, ROW)
+    sent(a_recv, COL)
+    sent(c_recv, COL + 1)
+    sent(st_recv.at[:, pl.ds(0, nd - 1)], ST)
+    sent(st_recv.at[:, pl.ds(0, nd - 1)], ST + 1)
+    sent(len_recv, LEN)
+    sent(row_recv.at[pl.ds(0, lots)], FIN)
+    gathers = 2 * layers
+    far, near_far = (ratio - 1) * nd, (ratio - 1) * (nd - 1)
+    aside_k, whole_k = gathers * MIXED, gathers * (lots - MIXED)
+    sent(x_recv.at[:, 0, pl.ds(0, (nd - 1) * chunk)], XF)
+    sent(y_recv.at[:, pl.ds(0, nd - 1)], YF)
+    sent(x_recv.at[pl.ds(0, whole_k), pl.ds(0, ratio - 1)], XF + 2)
+    sent(y_recv.at[pl.ds(0, whole_k), pl.ds(0, far)], YF + 2)
+    if MIXED:
+        sent(x_near.at[pl.ds(0, aside_k)], XF + 3)
+        sent(y_near.at[pl.ds(0, aside_k)], YF + 3)
+        sent(x_recv.at[pl.ds(0, aside_k), pl.ds(0, ratio - 1), pl.ds(0, (nd - 1) * chunk)], XF + 4)
+        sent(y_recv.at[pl.ds(0, aside_k), pl.ds(0, near_far)], YF + 4)
+
+    @pl.when(d != home)
+    def _():
+        sent(x_recv.at[:, 0, pl.ds(0, chunk)], XF + 1)
+        sent(y_recv.at[:, pl.ds(0, 1)], YF + 1)
+        if MIXED:
+            sent(x_recv.at[pl.ds(0, aside_k), pl.ds(0, ratio - 1), pl.ds(0, chunk)], XF + 5)
+            sent(y_recv.at[pl.ds(0, aside_k), pl.ds(0, ratio - 1)], YF + 5)
 
 
 def fused_shards(
@@ -628,14 +652,16 @@
         vm((layers, 2 * width, 2 * own_ch), bf16),
         vm((8, batch), f32),
         vm((n_row, nd, piece, cols), bf16),
-        vm((n_row, nd, piece, cols), bf16),
+        vm((n_row, nd - 1, piece, cols), bf16),
         vm((n_col, nd, lot, 2 * width), bf16),
-        vm((n_col, nd, lot, 2 * width), bf16),
+        vm((n_col, nd - 1, lot, 2 * width), bf16),
         vm((n_col, nd, half, 2 * width), bf16),
-        vm((n_col, nd, half, 2 * width), bf16),
+        vm((n_col, nd - 1, half, 2 * width), bf16),
         vm((n_all + lots, piece, cols), bf16),
+        vm((n_all, ratio - 1, piece, cols), bf16),
         vm((n_all, ratio, lot, cols), bf16),
         vm((n_all, half, 2 * width), bf16),
+        vm((n_all, ratio - 1, half, 2 * width), bf16),
         vm((n_all, nt, half, 2 * width), bf16),
         vm((layers, nd, 2, own, own_ch), f32),
         vm((layers, 2, batch, own_ch), f32),
@@ -644,19 +670,14 @@
         vm((rows, 128), f32),
         vm((steps * batch, 2 * width), bf16),
         vm((rows, 2 * width), bf16),
-        vm((nd, 8, batch), f32),
+        vm((nd - 1, 8, batch), f32),
         vm((rows, own * steps), bf16),
         vm((steps * batch, rows), bf16),
         dma((5, layers)), dma((3,)),
-        dma((n_row, nd)), dma((n_row, nd)),
-        dma((n_col, nd)), dma((n_col, nd)),
-        dma((n_col, nd)), dma((n_col, nd)),
-        dma((n_all, nd * ratio)), dma((n_all, nt)),
-        dma((n_all, nd * ratio)), dma((n_all, nt)),
-        dma((layers, nd)), dma((layers, nd)),
-        dma((layers, nd)), dma((layers, nd)),
-        dma((lots, nd)), dma((lots, nd)),
-        dma((nd,)), dma((nd,)),
+        dma((n_row,)), dma((n_col,)), dma((n_col,)),
+        dma((n_all, ratio)), dma((n_all, ratio)),
+        dma((n_all, ratio - 1)), dma((n_all, ratio - 1)),
+        dma((layers,)), dma((layers,)), dma((lots,)), dma((1,)), dma((LANES,)),
     ]
     inside = pl.BlockSpec(memory_space=pltpu.VMEM)
     outside = pl.BlockSpec(memory_space=pl.ANY)
@@ -703,7 +724,7 @@
 
     def run(*args):
         groups = args[8].shape[1] // ways
-        whole_groups = groups % nd == 0 and ways % nd == 0
+        whole_groups = groups % nd == 0 and ways % nd == 0 and ways > nd > 1
         body = fused_shards if whole_groups else shards
         return jax.shard_map(body, mesh=mesh, in_specs=in_specs, out_specs=out_specs, check_vma=False)(*args)
 

time: 155 us -> 145 us (0.935)
  Pallas kernels: 150 us -> 140 us
    pallas_call x1, Pallas kernels: 150 us -> 140 us  [fused_shards(): pl.pallas_call(functools.partial(fused_kernel, (layers, nd, nt, rows, mod...]
where the time goes in v2:
time: 145 us
  Pallas kernels  140 us (97%)
  local copies, waits for them, and re-layouts  3.55 us (2%)
    pallas_call x1, Pallas kernels, fused_shards(): pl.pallas_call(functools.partial(fused_kernel, (layers, nd, nt, rows, mod...  140 us
    unnamed x2, local copies, waits for them, and re-layouts  3.55 us

profile of v2, /device:TPU:0, one launch (start us, length us, event | category | flops | bytes accessed | tf_op | source)
XLA Modules:
  0.0 144.6 jit_solution(18037157342819508879)
XLA Ops:
  0.6 140.4 %shard_map.158 = (bf16[256,512]{1,0:T(8,128)(2,1)}, f32[2,2,32,1024]{3,2,1,0:T(8,128)}) custom-call(bf16[256,512]{1,0:T(8,128)(2,1)} %bitcast.6, s32[1,32]{1,0:T(1,128)} %bitcast.7, f32[2,4096]{1,0:T(2,128)} %gains.1, f32[2,16,64]{2,1,0:T(8,128)} %rate.1, f32[2,16,64]{2,1,0:T(8,128)} %turn.1, f32[2,16]{1,0:T(2,128)} %size.1, f32[2,2,16,16,64]{4,3,2,1,0:T(8,128)} %bitcast.4, ...), custom_call_target="tpu_custom_call" | custom-call | tf_op jit(solution)/shard_map/pallas_call | solution.py:684
  141.0 1.7 %copy.19 = bf16[32,8,512]{2,1,0:T(8,128)(2,1)} copy(bf16[32,8,512]{2,1,0:T(8,128)(2,1)} %bitcast.5) | data formatting | bytes 524288
  142.7 1.9 %copy.20 = f32[2,2,32,1024]{3,2,1,0:T(8,128)} copy(f32[2,2,32,1024]{3,2,1,0:T(8,128)} %get-tuple-element.9) | data formatting | bytes 1048576
